TPU v7x, 128 devices: a whole 4x4x4 slice. The times are simulated.
128 devices in a mesh: fs: 16 (over z, y), tp: 8 (over x, core).
Axes of the slice: x: 4, y: 4, z: 4, core: 2. Of those that a mesh axis runs over, the one named last changes fastest.
Arguments:
- stream: bfloat16 [16384, 1024], P(('fs', 'tp')), may hold values from -3 to 3
- mixer_out: bfloat16 [16384, 1024], P(('fs', 'tp')), may hold values from -6 to 6
- ffn_gains: float32 [4, 1024], replicated, may hold values from 0.5 to 1.5
- mixer_gain: float32 [1024], replicated, may hold values from 0.25 to 0.6
- gate_first: bfloat16 [1024, 2816], P('fs', 'tp'), may hold values from -0.1875 to 0.1875
- up_first: bfloat16 [1024, 2816], P('fs', 'tp'), may hold values from -0.1875 to 0.1875
- down_first: bfloat16 [2816, 1024], P('tp', 'fs'), may hold values from -0.109375 to 0.109375
- gate_second: bfloat16 [1024, 2816], P('fs', 'tp'), may hold values from -0.1875 to 0.1875
- up_second: bfloat16 [1024, 2816], P('fs', 'tp'), may hold values from -0.1875 to 0.1875
- down_second: bfloat16 [2816, 1024], P('tp', 'fs'), may hold values from -0.109375 to 0.109375
Outputs:
- layer_out: bfloat16 [16384, 1024], P(('fs', 'tp'))
All inputs are finite; a program needn't handle non-finite values.
Results may differ from a plain program's by a relative error of at most 0.02.
Values may be sent and summed in bfloat16 or wider, within the bound.
A program may use at most 64 MiB of HBM per device.

v0:
```python
import jax
import jax.numpy as jnp
from jax import lax
from jax.sharding import PartitionSpec as P

epsilon = 1e-06
half_weight = 0.5


def laid_out(blocks, dim):
    dims = list(blocks.shape[1:])
    dims[dim] *= blocks.shape[0]
    return jnp.moveaxis(blocks, 0, dim).reshape(dims)


def gather_together(arrays, axis, dims):
    line = jnp.concatenate([a.reshape(-1) for a in arrays])
    lines, at, gathered = (lax.all_gather(line, axis), 0, [])
    for a, dim in zip(arrays, dims):
        blocks = lines[:, at : at + a.size].reshape(-1, *a.shape)
        gathered.append(laid_out(blocks, dim))
        at += a.size
    return tuple(gathered)


def on_whole(shard, axis, dim, work):
    return work(lax.all_gather(shard, axis, axis=dim, tiled=True), jnp.int32(0))


def own_rows(portion, rows, axis):
    count = rows * lax.axis_size(axis)
    sent = portion(jnp.int32(0), count).astype(jnp.bfloat16)
    return lax.psum_scatter(sent, axis, scatter_dimension=0, tiled=True).astype(jnp.float32)


def rms_rows(values, gain_row):
    widened = values.astype(jnp.float32)
    inverse_rms = lax.rsqrt(jnp.mean(widened * widened, axis=-1, keepdims=True) + epsilon)
    return (widened * inverse_rms * gain_row.astype(jnp.float32)).astype(jnp.bfloat16)


def add_branch(rows, normed_branch, factor):
    return (rows.astype(jnp.float32) + factor * normed_branch.astype(jnp.float32)).astype(
        jnp.bfloat16
    )


def collect_weights(gate_local, up_local, down_local):
    gate_full, up_full = gather_together((gate_local, up_local), "fs", (0, 0))
    down_full = lax.all_gather(down_local, "fs", axis=1, tiled=True)
    return (gate_full, up_full, down_full)


def half_step(rows, gain_pre, gain_post, weight_set):
    gate_full, up_full, down_full = weight_set
    normed = rms_rows(rows, gain_pre)

    def activate(tokens_part, first_row):
        gate_sum = jnp.dot(tokens_part, gate_full, preferred_element_type=jnp.float32)
        up_sum = jnp.dot(tokens_part, up_full, preferred_element_type=jnp.float32)
        return (jax.nn.silu(gate_sum) * up_sum).astype(jnp.bfloat16)

    hidden = on_whole(normed, "tp", 0, activate)

    def project(first_row, row_count):
        row_block = lax.dynamic_slice_in_dim(hidden, first_row, row_count, 0)
        return jnp.dot(row_block, down_full, preferred_element_type=jnp.float32)

    branch = own_rows(project, normed.shape[0], "tp").astype(jnp.bfloat16)
    return add_branch(rows, rms_rows(branch, gain_post), half_weight)


def body(
    stream,
    mixer_out,
    ffn_gains,
    mixer_gain,
    gate_first,
    up_first,
    down_first,
    gate_second,
    up_second,
    down_second,
):
    first_set = collect_weights(gate_first, up_first, down_first)
    after_first = half_step(stream, ffn_gains[0], ffn_gains[1], first_set)
    mixed_in = add_branch(after_first, rms_rows(mixer_out, mixer_gain), 1.0)
    second_set = collect_weights(gate_second, up_second, down_second)
    return half_step(mixed_in, ffn_gains[2], ffn_gains[3], second_set)


def solution(mesh):
    placed = (
        P(("fs", "tp"), None),
        P(("fs", "tp"), None),
        P(),
        P(),
        P("fs", "tp"),
        P("fs", "tp"),
        P("tp", "fs"),
        P("fs", "tp"),
        P("fs", "tp"),
        P("tp", "fs"),
    )
    return jax.shard_map(
        body, mesh=mesh, in_specs=placed, out_specs=P(("fs", "tp"), None), check_vma=False
    )
```

profile of v0, /device:TPU:0, one launch (start us, length us, event | category | flops | bytes accessed | tf_op | source)
XLA Modules:
  0.0 245.0 jit_solution(8046702978109701361)
XLA Ops:
  9.1 1.1 fusion.13
  11.1 1.8 fusion.15
  14.0 28.4 %all_gather.27 = bf16[352,1024]{0,1:T(8,128)(2,1)} all-gather(bf16[352,64]{0,1:T(8,128)(2,1)S(1)} %copy-done.4), channel_id=1, replica_groups=mesh['fs'=16,'tp'=8] {'fs'}, dimensions={1}, use_global_device_ids=true | all-gather | bytes 765952 | tf_op jit(solution)/shard_map/all_gather | solution.py:50
  42.4 13.6 %all-gather.11.cloned.1.call-done = bf16[720896]{0:T(1024)(128)(2,1)} async-done(((bf16[45056]{0:T(1024)(128)(2,1)}), bf16[720896]{0:T(1024)(128)(2,1)}) %all-gather.11.cloned.1.call-update) | async-done | bytes 1441808 | tf_op jit(solution)/shard_map/all_gather | solution.py:18
  56.1 1.7 reshape.57
  57.9 1.2 reshape_reshape.12
  59.1 1.2 reshape_reshape.13
  60.3 22.0 %all-gather.7.cloned.1.call-done = bf16[1024,1024]{1,0:T(8,128)(2,1)} async-done(((bf16[128,1024]{1,0:T(8,128)(2,1)}), bf16[1024,1024]{1,0:T(8,128)(2,1)}) %all-gather.7.cloned.1.call-update) | async-done | bytes 2097168 | tf_op jit(solution)/shard_map/all_gather | solution.py:27
  82.3 3.7 %fusion.26 = f32[1024,352]{0,1:T(8,128)} fusion(bf16[1024,1024]{1,0:T(8,128)(2,1)} %all-gather.7.cloned.1.call-done, bf16[1024,352]{1,0:T(8,128)(2,1)S(1)} %reshape_reshape.12), kind=kOutput, calls=%fused_computation.50 | convolution fusion | flops 738197504 | bytes 4259840 | tf_op jit(solution)/shard_map/dot_general | solution.py:59
  86.0 5.6 %convolution_convert_fusion.1 = bf16[1024,1024]{1,0:T(8,128)(2,1)} fusion(bf16[352,1024]{0,1:T(8,128)(2,1)S(1)} %copy-done.3, bf16[1024,1024]{1,0:T(8,128)(2,1)} %all-gather.7.cloned.1.call-done, bf16[1024,352]{1,0:T(8,128)(2,1)S(1)} %reshape_reshape.13, f32[1024,352]{0,1:T(8,128)} %fusion.26), kind=kOutput, calls=%fused_computation.1 | convolution fusion | flops 1479606272 | bytes 7077888 | tf_op jit(solution)/shard_map/dot_general | solution.py:67
  92.7 27.5 %all_gather.31 = bf16[352,1024]{0,1:T(8,128)(2,1)} all-gather(bf16[352,64]{0,1:T(8,128)(2,1)S(1)} %copy-done.5), channel_id=1, replica_groups=mesh['fs'=16,'tp'=8] {'fs'}, dimensions={1}, use_global_device_ids=true | all-gather | bytes 765952 | tf_op jit(solution)/shard_map/all_gather | solution.py:50
  120.2 8.8 %all-gather.13.cloned.1.call-done = bf16[720896]{0:T(1024)(128)(2,1)} async-done(((bf16[45056]{0:T(1024)(128)(2,1)}), bf16[720896]{0:T(1024)(128)(2,1)}) %all-gather.13.cloned.1.call-update) | async-done | bytes 1441808 | tf_op jit(solution)/shard_map/all_gather | solution.py:18
  129.0 1.7 reshape.58
  130.7 33.2 %reduce-scatter.3.cloned.1.call-done = bf16[128,1024]{1,0:T(8,128)(2,1)} async-done(((bf16[1024,1024]{1,0:T(8,128)(2,1)}), bf16[128,1024]{1,0:T(8,128)(2,1)}) %reduce-scatter.3.cloned.1.call-update) | async-done | bytes 262160 | tf_op jit(solution)/shard_map/reduce_scatter | solution.py:33
  163.9 1.1 fusion.4
  165.0 1.3 fusion.17
  167.6 2.1 reshape_reshape.14
  169.6 1.2 reshape_reshape.15
  170.8 20.5 %all-gather.9.cloned.1.call-done = bf16[1024,1024]{1,0:T(8,128)(2,1)} async-done(((bf16[128,1024]{1,0:T(8,128)(2,1)}), bf16[1024,1024]{1,0:T(8,128)(2,1)}) %all-gather.9.cloned.1.call-update) | async-done | bytes 2097168 | tf_op jit(solution)/shard_map/all_gather | solution.py:27
  191.4 3.9 %fusion.27 = f32[1024,352]{0,1:T(8,128)} fusion(bf16[1024,1024]{1,0:T(8,128)(2,1)} %all-gather.9.cloned.1.call-done, bf16[1024,352]{1,0:T(8,128)(2,1)} %reshape_reshape.14), kind=kOutput, calls=%fused_computation.51 | convolution fusion | flops 738197504 | bytes 4259840 | tf_op jit(solution)/shard_map/dot_general | solution.py:59
  195.3 5.6 %convolution_convert_fusion = bf16[1024,1024]{1,0:T(8,128)(2,1)} fusion(bf16[352,1024]{0,1:T(8,128)(2,1)S(1)} %copy-done.2, bf16[1024,1024]{1,0:T(8,128)(2,1)} %all-gather.9.cloned.1.call-done, bf16[1024,352]{1,0:T(8,128)(2,1)S(1)} %reshape_reshape.15, f32[1024,352]{0,1:T(8,128)} %fusion.27), kind=kOutput, calls=%fused_computation | convolution fusion | flops 1479606272 | bytes 7077888 | tf_op jit(solution)/shard_map/dot_general | solution.py:67
  200.9 34.4 %reduce-scatter.5.cloned.1.call-done = bf16[128,1024]{1,0:T(8,128)(2,1)} async-done(((bf16[1024,1024]{1,0:T(8,128)(2,1)}), bf16[128,1024]{1,0:T(8,128)(2,1)}) %reduce-scatter.5.cloned.1.call-update) | async-done | bytes 262160 | tf_op jit(solution)/shard_map/reduce_scatter | solution.py:33
  235.2 1.1 fusion.10
  236.3 1.8 fusion.20
  (46 shorter events, 6.9 us)
Async XLA Ops:
  6.5 6.5 %copy-start.6 = (bf16[64,352]{1,0:T(8,128)(2,1)S(1)}, bf16[64,352]{1,0:T(8,128)(2,1)}, u32[]{:S(2)}) copy-start(bf16[64,352]{1,0:T(8,128)(2,1)} %param.17) | copy-start | bytes 135172
  6.5 6.6 %copy-start.7 = (bf16[64,352]{1,0:T(8,128)(2,1)S(1)}, bf16[64,352]{1,0:T(8,128)(2,1)}, u32[]{:S(2)}) copy-start(bf16[64,352]{1,0:T(8,128)(2,1)} %param.18) | copy-start | bytes 135172
  6.5 7.5 %copy-start.4 = (bf16[352,64]{0,1:T(8,128)(2,1)S(1)}, bf16[352,64]{0,1:T(8,128)(2,1)}, u32[]{:S(2)}) copy-start(bf16[352,64]{0,1:T(8,128)(2,1)} %param.16) | copy-start | bytes 135172
  6.5 49.5 %all-gather.11.cloned.1.call-start = ((), (), s32[]{:S(2)}) async-start(), calls=%async_computation.6 | async-start | bytes 1531904 | tf_op jit(solution)/shard_map/all_gather | solution.py:18
  9.1 73.2 %all-gather.7.cloned.1.call-start = ((), (), s32[]{:S(2)}) async-start(), calls=%async_computation.2 | async-start | bytes 2359296 | tf_op jit(solution)/shard_map/all_gather | solution.py:27
  12.9 116.0 %all-gather.13.cloned.1.call-start = ((), (), s32[]{:S(2)}) async-start(), calls=%async_computation.7 | async-start | bytes 1531904 | tf_op jit(solution)/shard_map/all_gather | solution.py:18
  13.9 150.0 %reduce-scatter.3.cloned.1.call-start = ((), (), s32[]{:S(2)}) async-start(), calls=%async_computation.3 | async-start | bytes 2359296 | tf_op jit(solution)/shard_map/reduce_scatter | solution.py:33
  60.3 25.7 %copy-start.3 = (bf16[352,1024]{0,1:T(8,128)(2,1)S(1)}, bf16[352,1024]{0,1:T(8,128)(2,1)}, u32[]{:S(2)}) copy-start(bf16[352,1024]{0,1:T(8,128)(2,1)} %all_gather.27) | copy-start | bytes 2162692
  91.6 0.9 copy-start.1
  91.6 1.1 copy-start.5
  91.6 99.8 %all-gather.9.cloned.1.call-start = ((), (), s32[]{:S(2)}) async-start(), calls=%async_computation.4 | async-start | bytes 2359296 | tf_op jit(solution)/shard_map/all_gather | solution.py:27
  120.1 44.8 %copy-start = (bf16[128,1024]{1,0:T(8,128)(2,1)S(1)}, bf16[128,1024]{1,0:T(8,128)(2,1)}, u32[]{:S(2)}) copy-start(bf16[128,1024]{1,0:T(8,128)(2,1)} %param.10) | copy-start | bytes 786436
  120.2 44.8 %copy-start.8 = (f32[1024]{0:T(1024)S(1)}, f32[1024]{0:T(1024)}, u32[]{:S(2)}) copy-start(f32[1024]{0:T(1024)} %param.13) | copy-start | bytes 12292
  167.2 68.0 %reduce-scatter.5.cloned.1.call-start = ((), (), s32[]{:S(2)}) async-start(), calls=%async_computation.5 | async-start | bytes 2359296 | tf_op jit(solution)/shard_map/reduce_scatter | solution.py:33
  170.8 24.4 %copy-start.2 = (bf16[352,1024]{0,1:T(8,128)(2,1)S(1)}, bf16[352,1024]{0,1:T(8,128)(2,1)}, u32[]{:S(2)}) copy-start(bf16[352,1024]{0,1:T(8,128)(2,1)} %all_gather.31) | copy-start | bytes 2162692
Sparse Core Ops, SparseCore 0:
  9.5 46.5 all-gather.10
  57.8 24.4 all-gather.6
  84.4 44.4 all-gather.12
  131.2 32.6 reduce-scatter.2
  167.3 23.9 all-gather.8
  201.0 34.1 reduce-scatter.4
where the time goes:
time: 246 us; the launch traced here: 245 us
  waiting for transfers between devices  133 us (54%)
  blocking collectives  55.9 us (23%)
  matrix products  18.7 us (8%)
  between operations  13.6 us (6%)
  local copies, waits for them, and re-layouts  13.3 us (5%)
  other arithmetic  10.5 us (4%)
    reduce_scatter x2, waiting for transfers between devices, own_rows(): lax.psum_scatter(sent, axis, scatter_dimension=0, tiled=True)  67.5 us
    all_gather x2, blocking collectives, collect_weights(): down_full = lax.all_gather(down_local, 'fs', axis=1, tiled=True)  55.9 us
    all_gather x2, waiting for transfers between devices, on_whole(): return work(lax.all_gather(shard, axis, axis=dim, tiled=True), jnp.int32(0))  42.5 us
    all_gather x2, waiting for transfers between devices, gather_together(): lines, at, gathered = (lax.all_gather(line, axis), 0, [])  22.4 us
    dot_general x2, matrix products, project(): return jnp.dot(row_block, down_full, preferred_element_type=jnp.float32)  11.2 us
    dot_general x2, matrix products, activate(): jnp.dot(tokens_part, gate_full, preferred_element_type=jnp.float32)  7.55 us
    another operation x4, local copies, waits for them, and re-layouts, laid_out(): return jnp.moveaxis(blocks, 0, dim).reshape(dims)  5.66 us
  transfers between devices with their start and end apart: 6, of which 6 were waited for; matrix products, arithmetic and copies ran while one was open for 10% of the time, Pallas kernels for 0%

commit v1 on v0

--- a/solution.py
+++ b/solution.py
@@ -47,7 +47,9 @@
 
 def collect_weights(gate_local, up_local, down_local):
     gate_full, up_full = gather_together((gate_local, up_local), "fs", (0, 0))
-    down_full = lax.all_gather(down_local, "fs", axis=1, tiled=True)
+    down_full = jnp.concatenate(
+        lax.all_to_all(jnp.stack([down_local] * lax.axis_size("fs")), "fs", 0, 0), axis=1
+    )
     return (gate_full, up_full, down_full)
 
 

time: 246 us -> 256 us (1.041)
  blocking collectives: 55.9 us -> 0 us
  waiting for transfers between devices: 133 us -> 181 us
  starting transfers between devices: 0.39 us -> 15.6 us
    all_gather x2 -> x0, blocking collectives: 55.9 us -> none  [collect_weights(): down_full = lax.all_gather(down_local, 'fs', axis=1, tiled=True)]
    all_gather x2, waiting for transfers between devices: 22.4 us -> 70.3 us  [gather_together(): lines, at, gathered = (lax.all_gather(line, axis), 0, [])]
    all_to_all x0 -> x2, starting transfers between devices: none -> 15.2 us  [collect_weights(): lax.all_to_all(jnp.stack([down_local] * lax.axis_size('fs')), 'fs', 0, 0)]
  transfers between devices with their start and end apart: 6 -> 8, of which waited for: 6 -> 6; matrix products, arithmetic and copies ran while one was open for 10% -> 13% of each run, Pallas kernels for 0% -> 0%
where the time goes in v1:
time: 256 us; the launch traced here: 255 us
  waiting for transfers between devices  181 us (71%)
  matrix products  19 us (7%)
  starting transfers between devices  15.6 us (6%)
  local copies, waits for them, and re-layouts  15.3 us (6%)
  between operations  13.6 us (5%)
  other arithmetic  10.5 us (4%)
    all_gather x2, waiting for transfers between devices, gather_together(): lines, at, gathered = (lax.all_gather(line, axis), 0, [])  70.3 us
    reduce_scatter x2, waiting for transfers between devices, own_rows(): lax.psum_scatter(sent, axis, scatter_dimension=0, tiled=True)  68 us
    all_gather x2, waiting for transfers between devices, on_whole(): return work(lax.all_gather(shard, axis, axis=dim, tiled=True), jnp.int32(0))  42.6 us
    all_to_all x2, starting transfers between devices, collect_weights(): lax.all_to_all(jnp.stack([down_local] * lax.axis_size('fs')), 'fs', 0, 0)  15.2 us
    dot_general x2, matrix products, project(): return jnp.dot(row_block, down_full, preferred_element_type=jnp.float32)  11.6 us
    dot_general x2, matrix products, activate(): jnp.dot(tokens_part, gate_full, preferred_element_type=jnp.float32)  7.39 us
    another operation x4, local copies, waits for them, and re-layouts, laid_out(): return jnp.moveaxis(blocks, 0, dim).reshape(dims)  5.67 us
  transfers between devices with their start and end apart: 8, of which 6 were waited for; matrix products, arithmetic and copies ran while one was open for 13% of the time, Pallas kernels for 0%

profile of v1, /device:TPU:0, one launch (start us, length us, event | category | flops | bytes accessed | tf_op | source)
XLA Modules:
  0.0 255.0 jit_solution(15520524956206022996)
XLA Ops:
  9.1 1.1 fusion.13
  11.1 1.8 fusion.15
  12.9 1.1 stack.4
  14.0 8.2 %all-to-all-start = ((bf16[16,352,64]{1,2,0:T(8,128)(2,1)}), bf16[16,352,64]{1,2,0:T(8,128)(2,1)}, u32[]{:S(2)}, u32[]{:S(2)}) async-start(bf16[16,352,64]{1,2,0:T(8,128)(2,1)} %stack.4), calls=%async_computation | async-start | bytes 1572864 | tf_op jit(solution)/shard_map/all_to_all | solution.py:51
  23.3 37.1 %all-gather.11.cloned.1.call-done = bf16[720896]{0:T(1024)(128)(2,1)} async-done(((bf16[45056]{0:T(1024)(128)(2,1)}), bf16[720896]{0:T(1024)(128)(2,1)}) %all-gather.11.cloned.1.call-update) | async-done | bytes 1441808 | tf_op jit(solution)/shard_map/all_gather | solution.py:18
  60.4 1.7 reshape.77
  62.2 1.2 reshape_reshape.12
  63.4 1.2 reshape_reshape.13
  64.6 22.0 %all-gather.7.cloned.1.call-done = bf16[1024,1024]{1,0:T(8,128)(2,1)} async-done(((bf16[128,1024]{1,0:T(8,128)(2,1)}), bf16[1024,1024]{1,0:T(8,128)(2,1)}) %all-gather.7.cloned.1.call-update) | async-done | bytes 2097168 | tf_op jit(solution)/shard_map/all_gather | solution.py:27
  86.6 3.7 %fusion.26 = f32[1024,352]{0,1:T(8,128)} fusion(bf16[1024,1024]{1,0:T(8,128)(2,1)} %all-gather.7.cloned.1.call-done, bf16[1024,352]{1,0:T(8,128)(2,1)S(1)} %reshape_reshape.12), kind=kOutput, calls=%fused_computation.50 | convolution fusion | flops 738197504 | bytes 4259840 | tf_op jit(solution)/shard_map/dot_general | solution.py:61
  90.3 5.8 %convolution_convert_fusion.1 = bf16[1024,1024]{1,0:T(8,128)(2,1)} fusion(bf16[352,1024]{0,1:T(8,128)(2,1)} %bitcast.2, bf16[1024,1024]{1,0:T(8,128)(2,1)} %all-gather.7.cloned.1.call-done, bf16[1024,352]{1,0:T(8,128)(2,1)S(1)} %reshape_reshape.13, f32[1024,352]{0,1:T(8,128)} %fusion.26), kind=kOutput, calls=%fused_computation.1 | convolution fusion | flops 1479606272 | bytes 7077888 | tf_op jit(solution)/shard_map/dot_general | solution.py:69
  97.9 7.0 %all-to-all-start.1 = ((bf16[16,352,64]{1,2,0:T(8,128)(2,1)}), bf16[16,352,64]{1,2,0:T(8,128)(2,1)}, u32[]{:S(2)}, u32[]{:S(2)}) async-start(bf16[16,352,64]{1,2,0:T(8,128)(2,1)} %stack.5), calls=%async_computation.2 | async-start | bytes 1572864 | tf_op jit(solution)/shard_map/all_to_all | solution.py:51
  105.2 33.2 %all-gather.13.cloned.1.call-done = bf16[720896]{0:T(1024)(128)(2,1)} async-done(((bf16[45056]{0:T(1024)(128)(2,1)}), bf16[720896]{0:T(1024)(128)(2,1)}) %all-gather.13.cloned.1.call-update) | async-done | bytes 1441808 | tf_op jit(solution)/shard_map/all_gather | solution.py:18
  138.4 1.7 reshape.78
  140.1 33.6 %reduce-scatter.3.cloned.1.call-done = bf16[128,1024]{1,0:T(8,128)(2,1)} async-done(((bf16[1024,1024]{1,0:T(8,128)(2,1)}), bf16[128,1024]{1,0:T(8,128)(2,1)}) %reduce-scatter.3.cloned.1.call-update) | async-done | bytes 262160 | tf_op jit(solution)/shard_map/reduce_scatter | solution.py:33
  173.8 1.1 fusion.4
  174.9 1.3 fusion.17
  177.4 2.1 reshape_reshape.14
  179.5 1.2 reshape_reshape.15
  180.7 20.6 %all-gather.9.cloned.1.call-done = bf16[1024,1024]{1,0:T(8,128)(2,1)} async-done(((bf16[128,1024]{1,0:T(8,128)(2,1)}), bf16[1024,1024]{1,0:T(8,128)(2,1)}) %all-gather.9.cloned.1.call-update) | async-done | bytes 2097168 | tf_op jit(solution)/shard_map/all_gather | solution.py:27
  201.3 3.7 %fusion.27 = f32[1024,352]{0,1:T(8,128)} fusion(bf16[1024,1024]{1,0:T(8,128)(2,1)} %all-gather.9.cloned.1.call-done, bf16[1024,352]{1,0:T(8,128)(2,1)S(1)} %copy-done.2), kind=kOutput, calls=%fused_computation.51 | convolution fusion | flops 738197504 | bytes 4259840 | tf_op jit(solution)/shard_map/dot_general | solution.py:61
  205.0 5.8 %convolution_convert_fusion = bf16[1024,1024]{1,0:T(8,128)(2,1)} fusion(bf16[352,1024]{0,1:T(8,128)(2,1)} %bitcast.6, bf16[1024,1024]{1,0:T(8,128)(2,1)} %all-gather.9.cloned.1.call-done, bf16[1024,352]{1,0:T(8,128)(2,1)S(1)} %reshape_reshape.15, f32[1024,352]{0,1:T(8,128)} %fusion.27), kind=kOutput, calls=%fused_computation | convolution fusion | flops 1479606272 | bytes 7077888 | tf_op jit(solution)/shard_map/dot_general | solution.py:69
  210.8 34.4 %reduce-scatter.5.cloned.1.call-done = bf16[128,1024]{1,0:T(8,128)(2,1)} async-done(((bf16[1024,1024]{1,0:T(8,128)(2,1)}), bf16[128,1024]{1,0:T(8,128)(2,1)}) %reduce-scatter.5.cloned.1.call-update) | async-done | bytes 262160 | tf_op jit(solution)/shard_map/reduce_scatter | solution.py:33
  246.3 1.8 fusion.20
  (48 shorter events, 8.9 us)
Async XLA Ops:
  6.5 6.4 %copy-start.3 = (bf16[352,64]{0,1:T(8,128)(2,1)S(1)}, bf16[352,64]{0,1:T(8,128)(2,1)}, u32[]{:S(2)}) copy-start(bf16[352,64]{0,1:T(8,128)(2,1)} %param.16) | copy-start | bytes 135172
  6.5 53.8 %all-gather.11.cloned.1.call-start = ((), (), s32[]{:S(2)}) async-start(), calls=%async_computation.8 | async-start | bytes 1531904 | tf_op jit(solution)/shard_map/all_gather | solution.py:18
  9.1 77.5 %all-gather.7.cloned.1.call-start = ((), (), s32[]{:S(2)}) async-start(), calls=%async_computation.4 | async-start | bytes 2359296 | tf_op jit(solution)/shard_map/all_gather | solution.py:27
  12.9 9.4 %copy-start.5 = (bf16[64,352]{1,0:T(8,128)(2,1)S(1)}, bf16[64,352]{1,0:T(8,128)(2,1)}, u32[]{:S(2)}) copy-start(bf16[64,352]{1,0:T(8,128)(2,1)} %param.17) | copy-start | bytes 135172
  12.9 9.5 %copy-start.6 = (bf16[64,352]{1,0:T(8,128)(2,1)S(1)}, bf16[64,352]{1,0:T(8,128)(2,1)}, u32[]{:S(2)}) copy-start(bf16[64,352]{1,0:T(8,128)(2,1)} %param.18) | copy-start | bytes 135172
  14.0 76.3 %all-to-all-start = ((bf16[16,352,64]{1,2,0:T(8,128)(2,1)}), bf16[16,352,64]{1,2,0:T(8,128)(2,1)}, u32[]{:S(2)}, u32[]{:S(2)}) async-start(bf16[16,352,64]{1,2,0:T(8,128)(2,1)} %stack.4), calls=%async_computation | async-start | bytes 1572864 | tf_op jit(solution)/shard_map/all_to_all | solution.py:51
  22.2 116.2 %all-gather.13.cloned.1.call-start = ((), (), s32[]{:S(2)}) async-start(), calls=%async_computation.9 | async-start | bytes 1531904 | tf_op jit(solution)/shard_map/all_gather | solution.py:18
  23.2 150.5 %reduce-scatter.3.cloned.1.call-start = ((), (), s32[]{:S(2)}) async-start(), calls=%async_computation.5 | async-start | bytes 2359296 | tf_op jit(solution)/shard_map/reduce_scatter | solution.py:33
  96.1 0.8 copy-start.4
  96.9 8.1 %copy-start.1 = (bf16[128,1024]{1,0:T(8,128)(2,1)S(1)}, bf16[128,1024]{1,0:T(8,128)(2,1)}, u32[]{:S(2)}) copy-start(bf16[128,1024]{1,0:T(8,128)(2,1)} %param.11) | copy-start | bytes 786436
  97.9 107.1 %all-to-all-start.1 = ((bf16[16,352,64]{1,2,0:T(8,128)(2,1)}), bf16[16,352,64]{1,2,0:T(8,128)(2,1)}, u32[]{:S(2)}, u32[]{:S(2)}) async-start(bf16[16,352,64]{1,2,0:T(8,128)(2,1)} %stack.5), calls=%async_computation.2 | async-start | bytes 1572864 | tf_op jit(solution)/shard_map/all_to_all | solution.py:51
  104.9 96.3 %all-gather.9.cloned.1.call-start = ((), (), s32[]{:S(2)}) async-start(), calls=%async_computation.6 | async-start | bytes 2359296 | tf_op jit(solution)/shard_map/all_gather | solution.py:27
  105.1 69.7 %copy-start = (bf16[128,1024]{1,0:T(8,128)(2,1)S(1)}, bf16[128,1024]{1,0:T(8,128)(2,1)}, u32[]{:S(2)}) copy-start(bf16[128,1024]{1,0:T(8,128)(2,1)} %param.10) | copy-start | bytes 786436
  105.2 69.7 %copy-start.7 = (f32[1024]{0:T(1024)S(1)}, f32[1024]{0:T(1024)}, u32[]{:S(2)}) copy-start(f32[1024]{0:T(1024)} %param.13) | copy-start | bytes 12292
  177.1 68.1 %reduce-scatter.5.cloned.1.call-start = ((), (), s32[]{:S(2)}) async-start(), calls=%async_computation.7 | async-start | bytes 2359296 | tf_op jit(solution)/shard_map/reduce_scatter | solution.py:33
  179.5 21.8 %copy-start.2 = (bf16[1024,352]{1,0:T(8,128)(2,1)S(1)}, bf16[1024,352]{1,0:T(8,128)(2,1)}, u32[]{:S(2)}) copy-start(bf16[1024,352]{1,0:T(8,128)(2,1)} %reshape_reshape.14) | copy-start | bytes 2162692
Sparse Core Ops, SparseCore 0:
  9.5 50.8 all-gather.10
  62.1 24.4 all-gather.6
  88.8 49.5 all-gather.12
  140.6 33.0 reduce-scatter.2
  177.2 24.0 all-gather.8
  210.9 34.2 reduce-scatter.4
